TPU v7x, 32 devices: a whole 2x2x4 slice. The times are simulated.
32 devices in a mesh: sp: 16 (over z, y, core), tp: 2 (over x).
Axes of the slice: x: 2, y: 2, z: 4, core: 2. Of those that a mesh axis runs over, the one named last changes fastest.
Arguments:
- query_rows: bfloat16 [8192, 1024], P(('sp', 'tp')), may hold values from -6 to 6
- key_rows: bfloat16 [8192, 1024], P(('sp', 'tp')), may hold values from -6 to 6
- value_rows: bfloat16 [8192, 1024], P(('sp', 'tp')), may hold values from -6 to 6
- out_grad: bfloat16 [8192, 1024], P(('sp', 'tp')), may hold values from -40 to 40
- log_totals: float32 [8192, 8], P(('sp', 'tp')), may hold values from 6 to 7.5
- out_dot: float32 [8192, 8], P(('sp', 'tp')), may hold values from -6 to 6
- bias_table: float32 [8, 320], replicated, may hold values from -4 to 4
Outputs:
- grad_query: bfloat16 [8192, 1024], P(('sp', 'tp'))
- grad_key: bfloat16 [8192, 1024], P(('sp', 'tp'))
- grad_value: bfloat16 [8192, 1024], P(('sp', 'tp'))
- grad_table: float32 [8, 320], replicated
All inputs are finite; a program needn't handle non-finite values.
Results may differ from a plain program's by a relative error of at most 0.005.
Values may be sent and summed in bfloat16 or wider, within the bound.
No kernel may reach another device: no remote copies, remote signals or barrier semaphores. Data moves between devices by JAX's collectives and lax.ppermute only.
A program may use at most 128 MiB of HBM per device.

v0:
```python
import jax
import jax.numpy as jnp
from jax import lax
from jax.sharding import PartitionSpec as P

SEG_LEN = 64
LEFT_SEGS = 8
REL_CLIP = 256


def passed_along(block, axis, distance):
    devices = range(lax.axis_size(axis))
    route = [(i - distance, i) for i in devices if i - distance in devices]
    return lax.ppermute(block, axis, route)


def band_matrix(diagonal_vals, row_count, col_count):
    head_count = diagonal_vals.shape[0]
    span_width = row_count + col_count - 1
    repeated = jnp.broadcast_to(diagonal_vals[:, None, :], (head_count, row_count, span_width))
    flat_rows = jnp.pad(
        repeated.reshape(head_count, row_count * span_width), ((0, 0), (0, row_count))
    )
    shaped = flat_rows.reshape(head_count, row_count, span_width + 1)[:, :, :col_count]
    return shaped[:, :, ::-1]


def diagonal_sums(matrix_vals):
    head_count, row_count, col_count = matrix_vals.shape
    span_width = row_count + col_count - 1
    flipped = jnp.pad(matrix_vals[:, :, ::-1], ((0, 0), (0, 0), (0, row_count)))
    skewed = flipped.reshape(head_count, row_count * (col_count + row_count))[
        :, : row_count * span_width
    ]
    return jnp.sum(skewed.reshape(head_count, row_count, span_width), axis=1)


def table_onehot(offset, row_count, col_count, table_len):
    diagonals = jnp.arange(row_count + col_count - 1, dtype=jnp.int32)
    distance = jnp.clip(offset + diagonals - (col_count - 1), 1 - SEG_LEN, REL_CLIP) + SEG_LEN - 1
    return (distance[:, None] == jnp.arange(table_len, dtype=jnp.int32)[None, :]).astype(
        jnp.float32
    )


def bias_block(bias_table, offset, row_count, col_count):
    onehot_map = table_onehot(offset, row_count, col_count, bias_table.shape[1])
    diagonal_vals = jnp.dot(bias_table, onehot_map.T, precision=lax.Precision.HIGHEST)
    return (band_matrix(diagonal_vals, row_count, col_count), onehot_map)


def band_stack(rows, block_count, span_segs):
    segmented = rows.reshape(-1, SEG_LEN, rows.shape[1])
    pieces = [segmented[start : start + block_count] for start in range(span_segs)]
    return jnp.stack(pieces, axis=1).reshape(block_count, span_segs * SEG_LEN, rows.shape[1])


def band_terms(queries, grads_out, log_rows, dot_rows, keys, values, bias_vals, allowed):
    block_count, query_count, feature_count = queries.shape
    key_count = keys.shape[1]
    head_count = log_rows.shape[2]
    query_heads = queries.reshape(block_count, query_count, head_count, -1)
    grad_heads = grads_out.reshape(block_count, query_count, head_count, -1)
    key_heads = keys.reshape(block_count, key_count, head_count, -1)
    value_heads = values.reshape(block_count, key_count, head_count, -1)
    inv_root = query_heads.shape[3] ** (-0.5)
    raw_scores = jnp.einsum(
        "bqhd,bkhd->bhqk", query_heads, key_heads, preferred_element_type=jnp.float32
    )
    scores = raw_scores * inv_root + bias_vals[None]
    log_terms = jnp.transpose(log_rows, (0, 2, 1))[:, :, :, None]
    dot_terms = jnp.transpose(dot_rows, (0, 2, 1))[:, :, :, None]
    weights = jnp.exp(scores - log_terms)
    weights = jnp.where(allowed[:, None, None, :], weights, 0.0)
    weight_grads = jnp.einsum(
        "bqhd,bkhd->bhqk", grad_heads, value_heads, preferred_element_type=jnp.float32
    )
    score_grads = weights * (weight_grads - dot_terms)
    return (
        weights.astype(jnp.bfloat16),
        score_grads.astype(jnp.bfloat16),
        score_grads,
        query_heads,
        key_heads,
        grad_heads,
        inv_root,
    )


def local(query_rows, key_rows, value_rows, out_grad, log_totals, out_dot, bias_table):
    row_count = query_rows.shape[0]
    feature_count = query_rows.shape[1]
    head_count = log_totals.shape[1]
    seg_count = row_count // SEG_LEN
    span_segs = LEFT_SEGS + 1
    band_len = span_segs * SEG_LEN
    need_rows = LEFT_SEGS * SEG_LEN
    lag_total = -(-need_rows // row_count)
    skip_rows = lag_total * row_count - need_rows
    first_row = lax.axis_index(("sp", "tp")) * row_count
    earlier = []
    for lag_count in range(lag_total, 0, -1):
        start_row = skip_rows if lag_count == lag_total else 0
        earlier.append(passed_along((key_rows, value_rows), ("sp", "tp"), lag_count))
    all_keys = jnp.concatenate([pair[0] for pair in earlier] + [key_rows], axis=0)
    all_values = jnp.concatenate([pair[1] for pair in earlier] + [value_rows], axis=0)
    key_bands = band_stack(all_keys, seg_count, span_segs)
    value_bands = band_stack(all_values, seg_count, span_segs)
    band_pos = (
        jnp.arange(seg_count, dtype=jnp.int32)[:, None] * SEG_LEN
        + jnp.arange(band_len, dtype=jnp.int32)[None, :]
    )
    allowed = first_row - need_rows + band_pos >= 0
    bias_vals, onehot_map = bias_block(bias_table, need_rows, SEG_LEN, band_len)
    weights_b, score_grads_b, score_grads, query_heads, key_heads, grad_heads, inv_root = (
        band_terms(
            query_rows.reshape(seg_count, SEG_LEN, feature_count),
            out_grad.reshape(seg_count, SEG_LEN, feature_count),
            log_totals.reshape(seg_count, SEG_LEN, head_count),
            out_dot.reshape(seg_count, SEG_LEN, head_count),
            key_bands,
            value_bands,
            bias_vals,
            allowed,
        )
    )
    tap_part = jnp.dot(
        diagonal_sums(jnp.sum(score_grads, axis=0)), onehot_map, precision=lax.Precision.HIGHEST
    )
    query_part = jnp.einsum(
        "bhqk,bkhd->bqhd", score_grads_b, key_heads, preferred_element_type=jnp.float32
    )
    grad_query = (query_part * inv_root).reshape(row_count, feature_count).astype(jnp.bfloat16)
    key_band_grad = jnp.einsum(
        "bhqk,bqhd->bkhd", score_grads_b, query_heads, preferred_element_type=jnp.float32
    )
    key_band_grad = (key_band_grad * inv_root).reshape(seg_count, span_segs, SEG_LEN, feature_count)
    value_band_grad = jnp.einsum(
        "bhqk,bqhd->bkhd", weights_b, grad_heads, preferred_element_type=jnp.float32
    )
    value_band_grad = value_band_grad.reshape(seg_count, span_segs, SEG_LEN, feature_count)
    key_all = sum(
        (
            jnp.pad(key_band_grad[:, lag], ((lag, LEFT_SEGS - lag), (0, 0), (0, 0)))
            for lag in range(span_segs)
        )
    ).reshape(-1, feature_count)
    value_all = sum(
        (
            jnp.pad(value_band_grad[:, lag], ((lag, LEFT_SEGS - lag), (0, 0), (0, 0)))
            for lag in range(span_segs)
        )
    ).reshape(-1, feature_count)
    key_total = key_all[need_rows:]
    value_total = value_all[need_rows:]
    for lag_count in range(1, lag_total + 1):
        lower_row = max(need_rows - lag_count * row_count, 0)
        upper_row = need_rows - (lag_count - 1) * row_count
        returned = passed_along(
            (key_all[lower_row:upper_row], value_all[lower_row:upper_row]), ("sp", "tp"), -lag_count
        )
        lead_rows = row_count - (upper_row - lower_row)
        key_total = key_total + returned[0]
        value_total = value_total + returned[1]
    grad_table = lax.psum(tap_part, ("sp", "tp"))
    return (
        grad_query,
        key_total.astype(jnp.bfloat16),
        value_total.astype(jnp.bfloat16),
        grad_table,
    )


def solution(mesh):
    placed = (
        P(("sp", "tp"), None),
        P(("sp", "tp"), None),
        P(("sp", "tp"), None),
        P(("sp", "tp"), None),
        P(("sp", "tp"), None),
        P(("sp", "tp"), None),
        P(),
    )
    return jax.shard_map(
        local,
        mesh=mesh,
        in_specs=placed,
        out_specs=(P(("sp", "tp"), None), P(("sp", "tp"), None), P(("sp", "tp"), None), P()),
        check_vma=False,
    )
```

profile of v0, /device:TPU:0, one launch (start us, length us, event | category | flops | bytes accessed | tf_op | source)
XLA Modules:
  0.0 198.3 jit_solution(5561602564015735739)
XLA Ops:
  0.6 5.7 %collective-permute-start.1 = (bf16[256,1024]{1,0:T(8,128)(2,1)}, bf16[256,1024]{1,0:T(8,128)(2,1)}, u32[]{:S(2)}, u32[]{:S(2)}) collective-permute-start(bf16[256,1024]{1,0:T(8,128)(2,1)} %param.8), channel_id=1, source_target_pairs={{0,1},{1,2},{2,3},{3,4},{4,5},{5,6},{6,7},{7,8},{8,9},{9,10},{10,1... | collective-permute-start | bytes 1572872 | tf_op jit(solution)/shard_map/ppermute | solution.py:14
  6.3 2.1 %collective-permute-start = (bf16[256,1024]{1,0:T(8,128)(2,1)}, bf16[256,1024]{1,0:T(8,128)(2,1)}, u32[]{:S(2)}, u32[]{:S(2)}) collective-permute-start(bf16[256,1024]{1,0:T(8,128)(2,1)} %param.8), channel_id=1, source_target_pairs={{0,2},{1,3},{2,4},{3,5},{4,6},{5,7},{6,8},{7,9},{8,10},{9,11},{10,... | collective-permute-start | bytes 1572872 | tf_op jit(solution)/shard_map/ppermute | solution.py:14
  8.4 4.1 %collective-permute-start.3 = (bf16[256,1024]{1,0:T(8,128)(2,1)}, bf16[256,1024]{1,0:T(8,128)(2,1)}, u32[]{:S(2)}, u32[]{:S(2)}) collective-permute-start(bf16[256,1024]{1,0:T(8,128)(2,1)} %param.9), channel_id=1, source_target_pairs={{0,1},{1,2},{2,3},{3,4},{4,5},{5,6},{6,7},{7,8},{8,9},{9,10},{10,1... | collective-permute-start | bytes 1572872 | tf_op jit(solution)/shard_map/ppermute | solution.py:14
  12.6 2.1 %collective-permute-start.2 = (bf16[256,1024]{1,0:T(8,128)(2,1)}, bf16[256,1024]{1,0:T(8,128)(2,1)}, u32[]{:S(2)}, u32[]{:S(2)}) collective-permute-start(bf16[256,1024]{1,0:T(8,128)(2,1)} %param.9), channel_id=1, source_target_pairs={{0,2},{1,3},{2,4},{3,5},{4,6},{5,7},{6,8},{7,9},{8,10},{9,11},{10,... | collective-permute-start | bytes 1572872 | tf_op jit(solution)/shard_map/ppermute | solution.py:14
  16.9 1.1 copy.172
  18.1 1.9 copy.175
  24.6 3.6 %collective-permute-done.3 = bf16[256,1024]{1,0:T(8,128)(2,1)} collective-permute-done((bf16[256,1024]{1,0:T(8,128)(2,1)}, bf16[256,1024]{1,0:T(8,128)(2,1)}, u32[]{:S(2)}, u32[]{:S(2)}) %collective-permute-start.3) | collective-permute-done | bytes 524320 | tf_op jit(solution)/shard_map/ppermute | solution.py:14
  28.2 1.2 constant_dynamic-update-slice_fusion.16
  30.0 1.2 constant_dynamic-update-slice_fusion.3
  34.1 1.2 copy.174
  37.8 1.2 copy.171
  39.1 1.7 fusion.5
  41.3 5.0 %convolution_bitcast_fusion = f32[4,576,8,128]{3,1,2,0:T(8,128)} fusion(f32[4,8,576,64]{2,3,1,0:T(8,128)S(1)} %fusion.5, f32[4,8,64]{2,1,0:T(8,128)S(1)} %get-tuple-element.49, f32[8,64,576]{2,1,0:T(8,128)S(1)} %slice.268, pred[4,576]{1,0:T(4,128)(4,1)S(1)} %add_compare_fusion, bf16[4,64,8,128]{3,2,1,0:T(8,128)(2,1)S(1)} %bitcast.221), kind=kOutput, calls=%fused_computation.13 | convolution fusion | flops 307888128 | bytes 15870208 | tf_op jit(solution)/shard_map/bhqk,bqhd->bkhd/dot_general | solution.py:138
  46.3 4.2 %fusion.52 = (f32[8,64,576]{2,1,0:T(8,128)S(1)}, bf16[4,8,64,576]{3,2,1,0:T(8,128)(2,1)}) fusion(f32[4,8,64]{2,1,0:T(8,128)S(1)} %get-tuple-element.48, bf16[4,64,8,128]{3,2,1,0:T(8,128)(2,1)S(1)} %bitcast.222, bf16[4,576,8,128]{3,2,1,0:T(8,128)(2,1)S(1)} %bitcast.220, f32[4,8,64]{2,1,0:T(8,128)S(1)} %get-tuple-element.49, f32[8,64,576]{2,1,0:T(8,128)S(1)} %slice.268, ...), kind=kOutput, calls=%fused_computation.101 | convolution fusion | flops 311132160 | bytes 14698752 | tf_op jit(solution)/shard_map/bqhd,bkhd->bhqk/dot_general | solution.py:75
  52.8 1.3 reshape.121
  54.2 12.8 %copy.146 = f32[4,576,8,128]{3,2,1,0:T(8,128)} copy(f32[4,576,8,128]{3,1,2,0:T(8,128)} %convolution_bitcast_fusion) | data formatting | bytes 18874368 | tf_op jit(solution)/shard_map/bhqk,bqhd->bkhd/transpose | solution.py:138
  67.0 11.2 %reshape.119 = f32[4,9,64,1024]{3,2,1,0:T(8,128)} reshape(f32[4,576,8,128]{3,2,1,0:T(8,128)} %copy.146) | data formatting | bytes 18874368 | tf_op jit(solution)/shard_map/reshape | solution.py:141
  78.2 4.7 %slice_bitcast_fusion.8 = (f32[4,64,1024]{2,1,0:T(8,128)S(1)}, f32[4,64,1024]{2,1,0:T(8,128)S(1)}, f32[4,64,1024]{2,1,0:T(8,128)S(1)}, f32[4,64,1024]{2,1,0:T(8,...) fusion(f32[4,9,64,1024]{3,2,1,0:T(8,128)} %reshape.119), kind=kLoop, calls=%fused_computation.37 | loop fusion | bytes 18874368 | tf_op jit(solution)/shard_map/squeeze | solution.py:150
  83.8 1.6 fusion.46
  85.5 1.3 collective-permute-start.7
  86.8 1.5 collective-permute-start.6
  88.3 1.5 multiply_bitcast_fusion
  89.8 9.1 %copy.136 = f32[4,576,8,128]{3,2,1,0:T(8,128)} copy(f32[4,576,8,128]{3,1,2,0:T(8,128)S(1)} %multiply_bitcast_fusion) | data formatting | bytes 18874368 | tf_op jit(solution)/shard_map/mul | solution.py:137
  98.9 11.1 %reshape.118 = f32[4,9,64,1024]{3,2,1,0:T(8,128)} reshape(f32[4,576,8,128]{3,2,1,0:T(8,128)} %copy.136) | data formatting | bytes 18874368 | tf_op jit(solution)/shard_map/reshape | solution.py:137
  110.0 4.7 %slice_bitcast_fusion.17 = (f32[4,64,1024]{2,1,0:T(8,128)S(1)}, f32[4,64,1024]{2,1,0:T(8,128)S(1)}, f32[4,64,1024]{2,1,0:T(8,128)S(1)}, f32[4,64,1024]{2,1,0:T(8...) fusion(f32[4,9,64,1024]{3,2,1,0:T(8,128)} %reshape.118), kind=kLoop, calls=%fused_computation.46 | loop fusion | bytes 18874368 | tf_op jit(solution)/shard_map/squeeze | solution.py:144
  115.8 1.7 fusion.47
  117.5 1.4 collective-permute-start.5
  118.9 1.3 collective-permute-start.4
  120.2 1.2 fusion.28
  123.2 70.2 %psum.7 = f32[8,320]{1,0:T(8,128)} all-reduce(f32[8,320]{1,0:T(8,128)S(1)} %fusion.37), channel_id=1, replica_groups=mesh['sp'=16,'tp'=2] {'sp','tp'}, use_global_device_ids=true, to_apply=%region_2.3 | all-reduce | flops 2560 | bytes 20480 | tf_op jit(solution)/shard_map/psum | solution.py:165
  193.4 2.6 %fusion.34 = bf16[256,1024]{1,0:T(8,128)(2,1)} fusion(f32[256,1024]{1,0:T(8,128)} %collective-permute-done.7, f32[256,1024]{1,0:T(8,128)} %collective-permute-done.6, f32[4,64,1024]{2,1,0:T(8,128)S(1)} %get-tuple-element.22), kind=kLoop, calls=%fused_computation.49 | loop fusion | flops 786432 | bytes 3670016 | tf_op jit(solution)/shard_map/convert_element_type | solution.py:169
  196.0 2.3 %fusion.36 = bf16[256,1024]{1,0:T(8,128)(2,1)} fusion(f32[256,1024]{1,0:T(8,128)S(1)} %collective-permute-done.5, f32[256,1024]{1,0:T(8,128)} %collective-permute-done.4, f32[4,64,1024]{2,1,0:T(8,128)S(1)} %get-tuple-element.25), kind=kLoop, calls=%fused_computation.52 | loop fusion | flops 786432 | bytes 3670016 | tf_op jit(solution)/shard_map/convert_element_type | solution.py:168
  (75 shorter events, 19.1 us)
Async XLA Ops:
  0.6 14.0 %copy-start = (f32[8,320]{1,0:T(8,128)S(1)}, f32[8,320]{1,0:T(8,128)}, u32[]{:S(2)}) copy-start(f32[8,320]{1,0:T(8,128)} %param.13) | copy-start | bytes 30724
  0.6 29.3 %collective-permute-start.1 = (bf16[256,1024]{1,0:T(8,128)(2,1)}, bf16[256,1024]{1,0:T(8,128)(2,1)}, u32[]{:S(2)}, u32[]{:S(2)}) collective-permute-start(bf16[256,1024]{1,0:T(8,128)(2,1)} %param.8), channel_id=1, source_target_pairs={{0,1},{1,2},{2,3},{3,4},{4,5},{5,6},{6,7},{7,8},{8,9},{9,10},{10,1... | collective-permute-start | bytes 1572872 | tf_op jit(solution)/shard_map/ppermute | solution.py:14
  6.3 17.2 %collective-permute-start = (bf16[256,1024]{1,0:T(8,128)(2,1)}, bf16[256,1024]{1,0:T(8,128)(2,1)}, u32[]{:S(2)}, u32[]{:S(2)}) collective-permute-start(bf16[256,1024]{1,0:T(8,128)(2,1)} %param.8), channel_id=1, source_target_pairs={{0,2},{1,3},{2,4},{3,5},{4,6},{5,7},{6,8},{7,9},{8,10},{9,11},{10,... | collective-permute-start | bytes 1572872 | tf_op jit(solution)/shard_map/ppermute | solution.py:14
  8.4 19.8 %collective-permute-start.3 = (bf16[256,1024]{1,0:T(8,128)(2,1)}, bf16[256,1024]{1,0:T(8,128)(2,1)}, u32[]{:S(2)}, u32[]{:S(2)}) collective-permute-start(bf16[256,1024]{1,0:T(8,128)(2,1)} %param.9), channel_id=1, source_target_pairs={{0,1},{1,2},{2,3},{3,4},{4,5},{5,6},{6,7},{7,8},{8,9},{9,10},{10,1... | collective-permute-start | bytes 1572872 | tf_op jit(solution)/shard_map/ppermute | solution.py:14
  12.6 9.9 %collective-permute-start.2 = (bf16[256,1024]{1,0:T(8,128)(2,1)}, bf16[256,1024]{1,0:T(8,128)(2,1)}, u32[]{:S(2)}, u32[]{:S(2)}) collective-permute-start(bf16[256,1024]{1,0:T(8,128)(2,1)} %param.9), channel_id=1, source_target_pairs={{0,2},{1,3},{2,4},{3,5},{4,6},{5,7},{6,8},{7,9},{8,10},{9,11},{10,... | collective-permute-start | bytes 1572872 | tf_op jit(solution)/shard_map/ppermute | solution.py:14
  22.0 7.4 %copy-start.6 = (bf16[256,1024]{1,0:T(8,128)(2,1)S(1)}, bf16[256,1024]{1,0:T(8,128)(2,1)}, u32[]{:S(2)}) copy-start(bf16[256,1024]{1,0:T(8,128)(2,1)} %param.9) | copy-start | bytes 1572868
  29.4 1.7 copy-start.7
  39.0 2.2 %copy-start.2 = (bf16[288,8,8,128]{3,2,1,0:T(8,128)(2,1)}, bf16[288,8,8,128]{3,2,1,0:T(8,128)(2,1)S(1)}, u32[]{:S(2)}) copy-start(bf16[288,8,8,128]{3,2,1,0:T(8,128)(2,1)S(1)} %copy.171) | copy-start | bytes 14155780
  39.1 2.2 %copy-start.5 = (bf16[32,8,8,128]{3,2,1,0:T(8,128)(2,1)S(1)}, bf16[32,8,8,128]{3,2,1,0:T(8,128)(2,1)}, u32[]{:S(2)}) copy-start(bf16[32,8,8,128]{3,2,1,0:T(8,128)(2,1)} %copy.175) | copy-start | bytes 1572868
  83.8 4.5 %copy-start.3 = (bf16[4,8,64,576]{3,2,1,0:T(8,128)(2,1)S(1)}, bf16[4,8,64,576]{3,2,1,0:T(8,128)(2,1)}, u32[]{:S(2)}) copy-start(bf16[4,8,64,576]{3,2,1,0:T(8,128)(2,1)} %get-tuple-element.45) | copy-start | bytes 7077892
  85.5 107.9 %collective-permute-start.7 = (f32[256,1024]{1,0:T(8,128)}, f32[256,1024]{1,0:T(8,128)}, u32[]{:S(2)}, u32[]{:S(2)}) collective-permute-start(f32[256,1024]{1,0:T(8,128)} %bitcast.67), channel_id=1, source_target_pairs={{2,0},{3,1},{4,2},{5,3},{6,4},{7,5},{8,6},{9,7},{10,8},{11,9},{12,... | collective-permute-start | bytes 3145736 | tf_op jit(solution)/shard_map/ppermute | solution.py:14
  86.8 106.6 %collective-permute-start.6 = (f32[256,1024]{1,0:T(8,128)}, f32[256,1024]{1,0:T(8,128)}, u32[]{:S(2)}, u32[]{:S(2)}) collective-permute-start(f32[256,1024]{1,0:T(8,128)} %bitcast.66), channel_id=1, source_target_pairs={{1,0},{2,1},{3,2},{4,3},{5,4},{6,5},{7,6},{8,7},{9,8},{10,9},{11,1... | collective-permute-start | bytes 3145736 | tf_op jit(solution)/shard_map/ppermute | solution.py:14
  110.0 10.2 %slice-start = ((s8[4718592]{0:T(1024)(128)(4,1)}), s8[524288]{0:T(1024)(128)(4,1)S(1)}, s32[]{:S(2)}) async-start(s8[4718592]{0:T(1024)(128)(4,1)} %bitcast.210), calls=%async_computation | async-start | bytes 1048576
  114.8 5.4 %slice-start.1 = ((s8[4718592]{0:T(1024)(128)(4,1)}), s8[4194304]{0:T(1024)(128)(4,1)S(1)}, s32[]{:S(2)}) async-start(s8[4718592]{0:T(1024)(128)(4,1)} %bitcast.210), calls=%async_computation.1 | async-start | bytes 8388608
  115.8 4.4 %copy-start.4 = (bf16[4,8,64,576]{3,2,1,0:T(8,128)(2,1)S(1)}, bf16[4,8,64,576]{3,2,1,0:T(8,128)(2,1)}, u32[]{:S(2)}) copy-start(bf16[4,8,64,576]{3,2,1,0:T(8,128)(2,1)} %get-tuple-element.45) | copy-start | bytes 7077892
  117.5 78.5 %collective-permute-start.5 = (f32[256,1024]{1,0:T(8,128)}, f32[256,1024]{1,0:T(8,128)S(1)}, u32[]{:S(2)}, u32[]{:S(2)}) collective-permute-start(f32[256,1024]{1,0:T(8,128)} %bitcast.54), channel_id=1, source_target_pairs={{2,0},{3,1},{4,2},{5,3},{6,4},{7,5},{8,6},{9,7},{10,8},{11,9},{12,... | collective-permute-start | bytes 3145736 | tf_op jit(solution)/shard_map/ppermute | solution.py:14
  118.9 77.1 %collective-permute-start.4 = (f32[256,1024]{1,0:T(8,128)}, f32[256,1024]{1,0:T(8,128)}, u32[]{:S(2)}, u32[]{:S(2)}) collective-permute-start(f32[256,1024]{1,0:T(8,128)} %bitcast.53), channel_id=1, source_target_pairs={{1,0},{2,1},{3,2},{4,3},{5,4},{6,5},{7,6},{8,7},{9,8},{10,9},{11,1... | collective-permute-start | bytes 3145736 | tf_op jit(solution)/shard_map/ppermute | solution.py:14
  120.2 78.0 %copy-start.1 = (f32[8,320]{1,0:T(8,128)S(1)}, f32[8,320]{1,0:T(8,128)}, u32[]{:S(2)}) copy-start(f32[8,320]{1,0:T(8,128)} %param.13) | copy-start | bytes 30724
where the time goes:
time: 200 us; the launch traced here: 198 us
  local copies, waits for them, and re-layouts  81.9 us (41%)
  blocking collectives  70.2 us (35%)
  starting transfers between devices  19.5 us (10%)
  matrix products  14.8 us (7%)
  other arithmetic  7.04 us (4%)
  waiting for transfers between devices  3.66 us (2%)
    psum x1, blocking collectives, local(): grad_table = lax.psum(tap_part, ('sp', 'tp'))  70.2 us
    unnamed x52, local copies, waits for them, and re-layouts  19.8 us
    ppermute x8, starting transfers between devices, passed_along(): return lax.ppermute(block, axis, route)  19.5 us
    transpose x1, local copies, waits for them, and re-layouts, local(): jnp.einsum('bhqk,bqhd->bkhd', weights_b, grad_heads, preferred_element_ty...  12.8 us
    reshape x1, local copies, waits for them, and re-layouts, local(): value_band_grad.reshape(seg_count, span_segs, SEG_LEN, feature_count)  11.2 us
    reshape x1, local copies, waits for them, and re-layouts, local(): (key_band_grad * inv_root).reshape(seg_count, span_segs, SEG_LEN, feature...  11.1 us
    mul x1, local copies, waits for them, and re-layouts, local(): key_band_grad * inv_root  9.13 us
    dot_general x1, matrix products, local(): jnp.einsum('bhqk,bqhd->bkhd', weights_b, grad_heads, preferred_element_ty...  5.01 us
  transfers between devices with their start and end apart: 8, of which 1 were waited for; matrix products, arithmetic and copies ran while one was open for 23% of the time, Pallas kernels for 0%

commit v1 on v0

--- a/solution.py
+++ b/solution.py
@@ -2,10 +2,16 @@
 import jax.numpy as jnp
 from jax import lax
 from jax.sharding import PartitionSpec as P
+from jax.lax import all_gather
 
 SEG_LEN = 64
 LEFT_SEGS = 8
 REL_CLIP = 256
+
+
+def drive_ratios(arr_in, axis_id):
+    vec_out = all_gather(arr_in, axis_id).sum(axis=0)
+    return vec_out
 
 
 def passed_along(block, axis, distance):
@@ -162,7 +168,7 @@
         lead_rows = row_count - (upper_row - lower_row)
         key_total = key_total + returned[0]
         value_total = value_total + returned[1]
-    grad_table = lax.psum(tap_part, ("sp", "tp"))
+    grad_table = drive_ratios(tap_part, ("sp", "tp"))
     return (
         grad_query,
         key_total.astype(jnp.bfloat16),

time: 200 us -> 227 us (1.14)
  blocking collectives: 70.2 us -> 92.8 us
  local copies, waits for them, and re-layouts: 81.9 us -> 85.7 us
  other arithmetic: 7.04 us -> 9.33 us
    all_gather x0 -> x1, blocking collectives: none -> 92.8 us  [drive_ratios(): vec_out = all_gather(arr_in, axis_id).sum(axis=0)]
    psum x1 -> x0, blocking collectives: 70.2 us -> none  [local(): grad_table = lax.psum(tap_part, ('sp', 'tp'))]
    unnamed x52 -> x70, local copies, waits for them, and re-layouts: 19.8 us -> 24.1 us
    transpose x1, local copies, waits for them, and re-layouts: 12.8 us -> 9.3 us  [local(): jnp.einsum('bhqk,bqhd->bkhd', weights_b, grad_heads, preferred_element_ty...]
    dot_general x1, matrix products: 5.01 us -> 2.39 us  [local(): jnp.einsum('bhqk,bqhd->bkhd', weights_b, grad_heads, preferred_element_ty...]
  transfers between devices with their start and end apart: 8 -> 8, of which waited for: 1 -> 1; matrix products, arithmetic and copies ran while one was open for 23% -> 25% of each run, Pallas kernels for 0% -> 0%
where the time goes in v1:
time: 227 us; the launch traced here: 225 us
  blocking collectives  92.8 us (41%)
  local copies, waits for them, and re-layouts  85.7 us (38%)
  starting transfers between devices  19.7 us (9%)
  matrix products  13.1 us (6%)
  other arithmetic  9.33 us (4%)
  waiting for transfers between devices  3.5 us (2%)
    all_gather x1, blocking collectives, drive_ratios(): vec_out = all_gather(arr_in, axis_id).sum(axis=0)  92.8 us
    unnamed x70, local copies, waits for them, and re-layouts  24.1 us
    ppermute x8, starting transfers between devices, passed_along(): return lax.ppermute(block, axis, route)  19.7 us
    reshape x1, local copies, waits for them, and re-layouts, local(): value_band_grad.reshape(seg_count, span_segs, SEG_LEN, feature_count)  11.1 us
    reshape x1, local copies, waits for them, and re-layouts, local(): (key_band_grad * inv_root).reshape(seg_count, span_segs, SEG_LEN, feature...  11.1 us
    transpose x1, local copies, waits for them, and re-layouts, local(): jnp.einsum('bhqk,bqhd->bkhd', weights_b, grad_heads, preferred_element_ty...  9.3 us
    mul x1, local copies, waits for them, and re-layouts, local(): key_band_grad * inv_root  9.12 us
    squeeze x1, local copies, waits for them, and re-layouts, local(): value_band_grad[:, lag]  6.41 us
  transfers between devices with their start and end apart: 8, of which 1 were waited for; matrix products, arithmetic and copies ran while one was open for 25% of the time, Pallas kernels for 0%

profile of v1, /device:TPU:0, one launch (start us, length us, event | category | flops | bytes accessed | tf_op | source)
XLA Modules:
  0.0 225.3 jit_solution(12074274174946755025)
XLA Ops:
  0.6 5.7 %collective-permute-start.1 = (bf16[256,1024]{1,0:T(8,128)(2,1)}, bf16[256,1024]{1,0:T(8,128)(2,1)}, u32[]{:S(2)}, u32[]{:S(2)}) collective-permute-start(bf16[256,1024]{1,0:T(8,128)(2,1)} %param.8), channel_id=1, source_target_pairs={{0,1},{1,2},{2,3},{3,4},{4,5},{5,6},{6,7},{7,8},{8,9},{9,10},{10,1... | collective-permute-start | bytes 1572872 | tf_op jit(solution)/shard_map/ppermute | solution.py:20
  6.3 2.1 collective-permute-start
  8.4 4.1 %collective-permute-start.3 = (bf16[256,1024]{1,0:T(8,128)(2,1)}, bf16[256,1024]{1,0:T(8,128)(2,1)}, u32[]{:S(2)}, u32[]{:S(2)}) collective-permute-start(bf16[256,1024]{1,0:T(8,128)(2,1)} %param.9), channel_id=1, source_target_pairs={{0,1},{1,2},{2,3},{3,4},{4,5},{5,6},{6,7},{7,8},{8,9},{9,10},{10,1... | collective-permute-start | bytes 1572872 | tf_op jit(solution)/shard_map/ppermute | solution.py:20
  12.6 2.1 collective-permute-start.2
  18.1 1.9 copy.175
  24.8 3.5 %collective-permute-done.3 = bf16[256,1024]{1,0:T(8,128)(2,1)} collective-permute-done((bf16[256,1024]{1,0:T(8,128)(2,1)}, bf16[256,1024]{1,0:T(8,128)(2,1)}, u32[]{:S(2)}, u32[]{:S(2)}) %collective-permute-start.3) | collective-permute-done | bytes 524320 | tf_op jit(solution)/shard_map/ppermute | solution.py:20
  33.9 3.4 %copy.174 = bf16[288,8,8,128]{3,2,1,0:T(8,128)(2,1)} copy(bf16[288,8,8,128]{3,1,2,0:T(8,128)(2,1)S(1)} %bitcast.217) | data formatting | bytes 9437184
  39.7 1.2 copy.171
  41.0 1.7 fusion.5
  43.1 2.3 %copy-done.2 = f32[4,8,576,64]{2,3,1,0:T(8,128)} copy-done((f32[4,8,576,64]{2,3,1,0:T(8,128)}, f32[4,8,576,64]{2,3,1,0:T(8,128)S(1)}, u32[]{:S(2)}) %copy-start.2) | copy-done | bytes 4718616
  45.4 2.4 %convolution_bitcast_fusion = f32[4,576,8,128]{3,1,2,0:T(8,128)S(1)} fusion(f32[4,8,576,64]{2,3,1,0:T(8,128)S(1)} %fusion.5, f32[4,8,64]{2,1,0:T(8,128)S(1)} %get-tuple-element.49, f32[8,64,576]{2,1,0:T(8,128)S(1)} %slice.268, pred[4,576]{1,0:T(4,128)(4,1)S(1)} %add_compare_fusion, bf16[4,64,8,128]{3,2,1,0:T(8,128)(2,1)S(1)} %bitcast.227), kind=kOutput, calls=%fused_computation.13 | convolution fusion | flops 307888128 | bytes 15870208 | tf_op jit(solution)/shard_map/bhqk,bqhd->bkhd/dot_general | solution.py:144
  47.8 9.3 %copy.146 = f32[4,576,8,128]{3,2,1,0:T(8,128)} copy(f32[4,576,8,128]{3,1,2,0:T(8,128)S(1)} %convolution_bitcast_fusion) | data formatting | bytes 18874368 | tf_op jit(solution)/shard_map/bhqk,bqhd->bkhd/transpose | solution.py:144
  57.1 11.1 %reshape.119 = f32[4,9,64,1024]{3,2,1,0:T(8,128)} reshape(f32[4,576,8,128]{3,2,1,0:T(8,128)} %copy.146) | data formatting | bytes 18874368 | tf_op jit(solution)/shard_map/reshape | solution.py:147
  68.2 6.4 %slice_bitcast_fusion.8 = (f32[4,64,1024]{2,1,0:T(8,128)S(1)}, f32[4,64,1024]{2,1,0:T(8,128)S(1)}, f32[4,64,1024]{2,1,0:T(8,128)S(1)}, f32[4,64,1024]{2,1,0:T(8,...) fusion(f32[4,9,64,1024]{3,2,1,0:T(8,128)} %reshape.119), kind=kLoop, calls=%fused_computation.37 | loop fusion | bytes 18874368 | tf_op jit(solution)/shard_map/squeeze | solution.py:156
  74.6 2.4 %pad_add_fusion = f32[12,64,1024]{2,1,0:T(8,128)S(1)} fusion(f32[4,64,1024]{2,1,0:T(8,128)} %get-tuple-element.11, f32[4,64,1024]{2,1,0:T(8,128)} %get-tuple-element.12, f32[4,64,1024]{2,1,0:T(8,128)S(1)} %get-tuple-element.5, f32[4,64,1024]{2,1,0:T(8,128)S(1)} %get-tuple-element.6, f32[4,64,1024]{2,1,0:T(8,128)S(1)} %get-tuple-element.7, ...), kind=kLoop, calls=%fused_computation.14 | loop fusion | flops 6291456 | bytes 12582912 | tf_op jit(solution)/shard_map/add | solution.py:154
  77.0 1.8 fusion.46
  78.8 1.3 collective-permute-start.7
  80.1 1.3 collective-permute-start.6
  81.4 4.4 %fusion.52 = (f32[8,64,576]{2,1,0:T(8,128)}, bf16[4,8,64,576]{3,2,1,0:T(8,128)(2,1)S(1)}) fusion(f32[4,8,64]{2,1,0:T(8,128)S(1)} %get-tuple-element.48, bf16[4,64,8,128]{3,2,1,0:T(8,128)(2,1)S(1)} %bitcast.228, bf16[4,576,8,128]{3,2,1,0:T(8,128)(2,1)S(1)} %bitcast.226, f32[4,8,64]{2,1,0:T(8,128)S(1)} %get-tuple-element.49, f32[8,64,576]{2,1,0:T(8,128)S(1)} %slice.268, ...), kind=kOutput, calls=%fused_computation.102 | convolution fusion | flops 311132160 | bytes 14698752 | tf_op jit(solution)/shard_map/bqhd,bkhd->bhqk/dot_general | solution.py:81
  85.8 1.5 multiply_bitcast_fusion
  87.3 9.1 %copy.136 = f32[4,576,8,128]{3,2,1,0:T(8,128)} copy(f32[4,576,8,128]{3,1,2,0:T(8,128)S(1)} %multiply_bitcast_fusion) | data formatting | bytes 18874368 | tf_op jit(solution)/shard_map/mul | solution.py:143
  96.4 11.1 %reshape.118 = f32[4,9,64,1024]{3,2,1,0:T(8,128)} reshape(f32[4,576,8,128]{3,2,1,0:T(8,128)} %copy.136) | data formatting | bytes 18874368 | tf_op jit(solution)/shard_map/reshape | solution.py:143
  107.5 4.7 %slice_bitcast_fusion.17 = (f32[4,64,1024]{2,1,0:T(8,128)S(1)}, f32[4,64,1024]{2,1,0:T(8,128)S(1)}, f32[4,64,1024]{2,1,0:T(8,128)S(1)}, f32[4,64,1024]{2,1,0:T(8...) fusion(f32[4,9,64,1024]{3,2,1,0:T(8,128)} %reshape.118), kind=kLoop, calls=%fused_computation.46 | loop fusion | bytes 18874368 | tf_op jit(solution)/shard_map/squeeze | solution.py:150
  113.3 1.8 fusion.47
  115.0 1.4 collective-permute-start.5
  116.5 1.7 collective-permute-start.4
  118.2 2.0 fusion.28
  122.3 1.3 reshape.121
  123.8 1.5 copy.134
  126.7 92.8 %all-gather = f32[256,320]{1,0:T(8,128)S(1)} all-gather(f32[8,320]{1,0:T(8,128)S(1)} %fusion.37), channel_id=2, replica_groups=mesh['sp'=16,'tp'=2] {'sp','tp'}, dimensions={0}, use_global_device_ids=true | all-gather | bytes 337920 | tf_op jit(solution)/shard_map/all_gather | solution.py:13
  220.1 2.6 %fusion.34 = bf16[256,1024]{1,0:T(8,128)(2,1)} fusion(f32[256,1024]{1,0:T(8,128)} %collective-permute-done.7, f32[256,1024]{1,0:T(8,128)} %collective-permute-done.6, f32[4,64,1024]{2,1,0:T(8,128)S(1)} %copy-done.4), kind=kLoop, calls=%fused_computation.49 | loop fusion | flops 786432 | bytes 3670016 | tf_op jit(solution)/shard_map/convert_element_type | solution.py:175
  222.7 2.6 %fusion.36 = bf16[256,1024]{1,0:T(8,128)(2,1)} fusion(f32[256,1024]{1,0:T(8,128)} %collective-permute-done.5, f32[256,1024]{1,0:T(8,128)} %collective-permute-done.4, f32[4,64,1024]{2,1,0:T(8,128)S(1)} %copy-done.5), kind=kLoop, calls=%fused_computation.52 | loop fusion | flops 786432 | bytes 3670016 | tf_op jit(solution)/shard_map/convert_element_type | solution.py:174
  (96 shorter events, 21.6 us)
Async XLA Ops:
  0.6 14.0 %copy-start = (f32[8,320]{1,0:T(8,128)S(1)}, f32[8,320]{1,0:T(8,128)}, u32[]{:S(2)}) copy-start(f32[8,320]{1,0:T(8,128)} %param.13) | copy-start | bytes 30724
  0.6 29.2 %collective-permute-start.1 = (bf16[256,1024]{1,0:T(8,128)(2,1)}, bf16[256,1024]{1,0:T(8,128)(2,1)}, u32[]{:S(2)}, u32[]{:S(2)}) collective-permute-start(bf16[256,1024]{1,0:T(8,128)(2,1)} %param.8), channel_id=1, source_target_pairs={{0,1},{1,2},{2,3},{3,4},{4,5},{5,6},{6,7},{7,8},{8,9},{9,10},{10,1... | collective-permute-start | bytes 1572872 | tf_op jit(solution)/shard_map/ppermute | solution.py:20
  6.3 17.4 %collective-permute-start = (bf16[256,1024]{1,0:T(8,128)(2,1)}, bf16[256,1024]{1,0:T(8,128)(2,1)}, u32[]{:S(2)}, u32[]{:S(2)}) collective-permute-start(bf16[256,1024]{1,0:T(8,128)(2,1)} %param.8), channel_id=1, source_target_pairs={{0,2},{1,3},{2,4},{3,5},{4,6},{5,7},{6,8},{7,9},{8,10},{9,11},{10,... | collective-permute-start | bytes 1572872 | tf_op jit(solution)/shard_map/ppermute | solution.py:20
  8.4 19.8 %collective-permute-start.3 = (bf16[256,1024]{1,0:T(8,128)(2,1)}, bf16[256,1024]{1,0:T(8,128)(2,1)}, u32[]{:S(2)}, u32[]{:S(2)}) collective-permute-start(bf16[256,1024]{1,0:T(8,128)(2,1)} %param.9), channel_id=1, source_target_pairs={{0,1},{1,2},{2,3},{3,4},{4,5},{5,6},{6,7},{7,8},{8,9},{9,10},{10,1... | collective-permute-start | bytes 1572872 | tf_op jit(solution)/shard_map/ppermute | solution.py:20
  12.6 10.0 %collective-permute-start.2 = (bf16[256,1024]{1,0:T(8,128)(2,1)}, bf16[256,1024]{1,0:T(8,128)(2,1)}, u32[]{:S(2)}, u32[]{:S(2)}) collective-permute-start(bf16[256,1024]{1,0:T(8,128)(2,1)} %param.9), channel_id=1, source_target_pairs={{0,2},{1,3},{2,4},{3,5},{4,6},{5,7},{6,8},{7,9},{8,10},{9,11},{10,... | collective-permute-start | bytes 1572872 | tf_op jit(solution)/shard_map/ppermute | solution.py:20
  22.2 7.2 %copy-start.10 = (bf16[256,1024]{1,0:T(8,128)(2,1)S(1)}, bf16[256,1024]{1,0:T(8,128)(2,1)}, u32[]{:S(2)}) copy-start(bf16[256,1024]{1,0:T(8,128)(2,1)} %param.9) | copy-start | bytes 1572868
  29.4 1.6 copy-start.11
  41.0 2.1 copy-start.3
  41.0 4.4 %copy-start.8 = (bf16[32,8,8,128]{3,2,1,0:T(8,128)(2,1)S(1)}, bf16[32,8,8,128]{3,2,1,0:T(8,128)(2,1)}, u32[]{:S(2)}) copy-start(bf16[32,8,8,128]{3,2,1,0:T(8,128)(2,1)} %copy.175) | copy-start | bytes 1572868
  43.1 2.3 %copy-start.2 = (f32[4,8,576,64]{2,3,1,0:T(8,128)}, f32[4,8,576,64]{2,3,1,0:T(8,128)S(1)}, u32[]{:S(2)}) copy-start(f32[4,8,576,64]{2,3,1,0:T(8,128)S(1)} %fusion.5) | copy-start | bytes 14155780
  68.2 13.2 %slice-start = ((s8[5242880]{0:T(1024)(128)(4,1)}), s8[4194304]{0:T(1024)(128)(4,1)S(1)}, s32[]{:S(2)}) async-start(s8[5242880]{0:T(1024)(128)(4,1)} %bitcast.211), calls=%async_computation | async-start | bytes 8388608
  68.2 13.2 %slice-start.4 = ((s8[4718592]{0:T(1024)(128)(4,1)}), s8[4194304]{0:T(1024)(128)(4,1)S(1)}, s32[]{:S(2)}) async-start(s8[4718592]{0:T(1024)(128)(4,1)} %bitcast.224), calls=%async_computation.4 | async-start | bytes 8388608
  74.6 6.8 %slice-start.1 = ((s8[5242880]{0:T(1024)(128)(4,1)}), s8[1048576]{0:T(1024)(128)(4,1)S(1)}, s32[]{:S(2)}) async-start(s8[5242880]{0:T(1024)(128)(4,1)} %bitcast.211), calls=%async_computation.1 | async-start | bytes 2097152
  74.6 6.8 %slice-start.5 = ((s8[4718592]{0:T(1024)(128)(4,1)}), s8[524288]{0:T(1024)(128)(4,1)S(1)}, s32[]{:S(2)}) async-start(s8[4718592]{0:T(1024)(128)(4,1)} %bitcast.224), calls=%async_computation.5 | async-start | bytes 1048576
  77.0 4.4 %copy-start.9 = (bf16[32,8,8,128]{3,2,1,0:T(8,128)(2,1)S(1)}, bf16[32,8,8,128]{3,2,1,0:T(8,128)(2,1)}, u32[]{:S(2)}) copy-start(bf16[32,8,8,128]{3,2,1,0:T(8,128)(2,1)} %copy.175) | copy-start | bytes 1572868
  78.8 141.3 %collective-permute-start.7 = (f32[256,1024]{1,0:T(8,128)}, f32[256,1024]{1,0:T(8,128)}, u32[]{:S(2)}, u32[]{:S(2)}) collective-permute-start(f32[256,1024]{1,0:T(8,128)} %bitcast.67), channel_id=1, source_target_pairs={{2,0},{3,1},{4,2},{5,3},{6,4},{7,5},{8,6},{9,7},{10,8},{11,9},{12,... | collective-permute-start | bytes 3145736 | tf_op jit(solution)/shard_map/ppermute | solution.py:20
  80.1 140.1 %collective-permute-start.6 = (f32[256,1024]{1,0:T(8,128)}, f32[256,1024]{1,0:T(8,128)}, u32[]{:S(2)}, u32[]{:S(2)}) collective-permute-start(f32[256,1024]{1,0:T(8,128)} %bitcast.66), channel_id=1, source_target_pairs={{1,0},{2,1},{3,2},{4,3},{5,4},{6,5},{7,6},{8,7},{9,8},{10,9},{11,1... | collective-permute-start | bytes 3145736 | tf_op jit(solution)/shard_map/ppermute | solution.py:20
  85.8 1.5 copy-start.6
  107.5 10.7 %slice-start.2 = ((s8[4718592]{0:T(1024)(128)(4,1)}), s8[524288]{0:T(1024)(128)(4,1)S(1)}, s32[]{:S(2)}) async-start(s8[4718592]{0:T(1024)(128)(4,1)} %bitcast.214), calls=%async_computation.2 | async-start | bytes 1048576
  112.2 5.9 %slice-start.3 = ((s8[4718592]{0:T(1024)(128)(4,1)}), s8[4194304]{0:T(1024)(128)(4,1)S(1)}, s32[]{:S(2)}) async-start(s8[4718592]{0:T(1024)(128)(4,1)} %bitcast.214), calls=%async_computation.3 | async-start | bytes 8388608
  113.3 4.9 %copy-start.7 = (bf16[4,8,64,576]{3,2,1,0:T(8,128)(2,1)S(1)}, bf16[4,8,64,576]{3,2,1,0:T(8,128)(2,1)}, u32[]{:S(2)}) copy-start(bf16[4,8,64,576]{3,2,1,0:T(8,128)(2,1)} %copy-done.6) | copy-start | bytes 7077892
  115.0 107.6 %collective-permute-start.5 = (f32[256,1024]{1,0:T(8,128)}, f32[256,1024]{1,0:T(8,128)}, u32[]{:S(2)}, u32[]{:S(2)}) collective-permute-start(f32[256,1024]{1,0:T(8,128)} %bitcast.54), channel_id=1, source_target_pairs={{2,0},{3,1},{4,2},{5,3},{6,4},{7,5},{8,6},{9,7},{10,8},{11,9},{12,... | collective-permute-start | bytes 3145736 | tf_op jit(solution)/shard_map/ppermute | solution.py:20
  116.5 3.8 %copy-start.12 = (f32[8,64,576]{2,1,0:T(8,128)S(1)}, f32[8,64,576]{2,1,0:T(8,128)}, u32[]{:S(2)}) copy-start(f32[8,64,576]{2,1,0:T(8,128)} %get-tuple-element.44) | copy-start | bytes 3538948
  116.5 106.2 %collective-permute-start.4 = (f32[256,1024]{1,0:T(8,128)}, f32[256,1024]{1,0:T(8,128)}, u32[]{:S(2)}, u32[]{:S(2)}) collective-permute-start(f32[256,1024]{1,0:T(8,128)} %bitcast.53), channel_id=1, source_target_pairs={{1,0},{2,1},{3,2},{4,3},{5,4},{6,5},{7,6},{8,7},{9,8},{10,9},{11,1... | collective-permute-start | bytes 3145736 | tf_op jit(solution)/shard_map/ppermute | solution.py:20
  123.6 96.5 %copy-start.4 = (f32[4,64,1024]{2,1,0:T(8,128)S(1)}, f32[4,64,1024]{2,1,0:T(8,128)}, u32[]{:S(2)}) copy-start(f32[4,64,1024]{2,1,0:T(8,128)} %get-tuple-element.22) | copy-start | bytes 3145732
  123.7 99.1 %copy-start.5 = (f32[4,64,1024]{2,1,0:T(8,128)S(1)}, f32[4,64,1024]{2,1,0:T(8,128)}, u32[]{:S(2)}) copy-start(f32[4,64,1024]{2,1,0:T(8,128)} %get-tuple-element.25) | copy-start | bytes 3145732
  125.3 100.0 %copy-start.1 = (f32[8,320]{1,0:T(8,128)S(1)}, f32[8,320]{1,0:T(8,128)}, u32[]{:S(2)}) copy-start(f32[8,320]{1,0:T(8,128)} %param.13) | copy-start | bytes 30724
